TPU v7x, 32 devices: a whole 2x2x4 slice. The times are simulated.
32 devices in a mesh: fs: 8 (over z, y), tp: 4 (over x, core).
Axes of the slice: x: 2, y: 2, z: 4, core: 2. Of those that a mesh axis runs over, the one named last changes fastest.
Arguments:
- tokens: bfloat16 [12288, 2048], P('fs', 'tp'), may hold values from -6 to 6
- norm_gain: float32 [2048], P('fs'), may hold values from 0.1 to 1.9
- up_weight: float32 [2048, 8192], P('fs', 'tp'), may hold values from -0.125 to 0.125
- down_weight: float32 [2048, 8192], P('fs', 'tp'), may hold values from -0.0625 to 0.0625
Outputs:
- up_matrix: bfloat16 [2048, 8192], P(None, 'tp')
- down_matrix: bfloat16 [2048, 8192], P(None, 'tp')
- mixed: bfloat16 [12288, 2048], P('fs', 'tp')
All inputs are finite; a program needn't handle non-finite values.
Results may differ from a plain program's by a relative error of at most 0.0095.
Values may be sent and summed in bfloat16 or wider, within the bound.
A program may use at most 128 MiB of HBM per device.

v0:
```python
import functools

import jax
import jax.numpy as jnp
from jax import lax
from jax.experimental import pallas as pl
from jax.experimental.pallas import tpu as pltpu
from jax.sharding import PartitionSpec as P

epsilon = 1e-06
MESH = pl.DeviceIdType.MESH
UP, DOWN, SIDE = 0, 1, 2


def chunks_of(rows, m):
    extra = max(16, rows * (2 + m) // 16 // 16 * 16)
    main, half = rows - extra, rows // 2
    if half % 128 == 0:
        return [(0, half), (half, main - half), (main, extra)]
    return [(0, main), (main, extra)]


def kernel(n, tp, tok_in, gain, up_weight, down_weight, up, down, total,
           stage, tok, hidden, part, pair, cross,
           send_sem, recv_sem, tok_send, tok_recv, pair_send, pair_recv, cross_send, cross_recv, local_sem):
    rows, units = up_weight.shape
    tokens, width = tok_in.shape
    chain = n // 2
    groups = tp // 2
    per_owner = n // tp
    chunks = [chunks_of(rows, 0), chunks_of(rows, 1)]
    extra = len(chunks[0]) - 1
    mains = range(extra)
    halves = extra
    half_rows = rows // halves
    fs, me = lax.axis_index("fs"), lax.axis_index("tp")
    z, y = fs // 2, fs % 2
    group, core = me // 2, me % 2
    partner = group * 2 + 1 - core
    bufs = (up, down)

    def target(way):
        if way == UP:
            return {"fs": jnp.minimum(z + 1, chain - 1) * 2 + y}
        if way == DOWN:
            return {"fs": jnp.maximum(z - 1, 0) * 2 + y}
        return {"fs": z * 2 + 1 - y}

    def spot(m, src, k):
        return pl.ds(pl.multiple_of(pl.multiple_of(src * rows, 16) + chunks[m][k][0], 16), chunks[m][k][1])

    def copy(m, src, k, way):
        where = spot(m, src, k)
        return pltpu.make_async_remote_copy(
            src_ref=bufs[m].at[where],
            dst_ref=bufs[m].at[where],
            send_sem=send_sem.at[m, way, src, k],
            recv_sem=recv_sem.at[m, src, k],
            device_id=target(way),
            device_id_type=MESH,
        )

    def arrived(m, src, k):
        where = spot(m, src, k)
        pltpu.make_async_remote_copy(
            src_ref=bufs[m].at[where], dst_ref=bufs[m].at[where],
            send_sem=send_sem.at[m, SIDE, src, k], recv_sem=recv_sem.at[m, src, k],
            device_id=target(SIDE), device_id_type=MESH,
        ).wait_recv()

    def own_sends(m):
        order = [(SIDE, extra)] + [(way, k) for k in mains for way in (UP, DOWN, SIDE)] + [(UP, extra), (DOWN, extra)]
        return [(way, k) for way, k in order]

    def when_way(way, fn):
        if way == UP:
            pl.when(z < chain - 1)(fn)
        elif way == DOWN:
            pl.when(z > 0)(fn)
        else:
            fn()

    def start_own(m):
        for way, k in own_sends(m):
            when_way(way, lambda way=way, k=k: copy(m, fs, k, way).start())

    def relay_own_extra(m, act):
        other = z * 2 + 1 - y
        for way in (UP, DOWN):
            when_way(way, lambda way=way: act(copy(m, other, extra, way)))

    def step_sends(m, d, act, wait):
        plan = [(k, 0) for k in mains] + [(extra, 0), (extra, 1)]
        for k, flip in plan:
            for sign, way in ((-1, UP), (1, DOWN)):
                at = z + sign * d
                src = at * 2 + (y + flip) % 2

                @pl.when((at >= 0) & (at < chain))
                def _():
                    if wait:
                        arrived(m, src, k)
                    when_way(way, lambda: act(copy(m, src, k, way)))
                    if k != extra:
                        act(copy(m, src, k, SIDE))

    def side_arrivals(m, d):
        for sign in (-1, 1) if not (isinstance(d, int) and d == 0) else (1,):
            at = z + sign * d

            @pl.when((at >= 0) & (at < chain))
            def _():
                for k in mains:
                    arrived(m, at * 2 + 1 - y, k)

    own_rows = pl.ds(pl.multiple_of(fs * rows, 16), rows)
    loads = [pltpu.make_async_copy(up_weight, stage.at[0], local_sem.at[1]),
             pltpu.make_async_copy(tok_in, tok.at[:, pl.ds(pl.multiple_of(me * width, 128), width)], local_sem.at[0]),
             pltpu.make_async_copy(down_weight, stage.at[1], local_sem.at[2])]
    for load in loads:
        load.start()

    barrier = pltpu.get_barrier_semaphore()
    greet = [{"fs": lax.rem(z + 1, chain) * 2 + y}, {"fs": lax.rem(z + chain - 1, chain) * 2 + y},
             {"fs": z * 2 + 1 - y}, {"tp": partner}]
    greet += [{"tp": lax.rem(group + g, groups) * 2 + core} for g in range(1, groups)]
    for who in greet:
        pl.semaphore_signal(barrier, inc=1, device_id=who, device_id_type=MESH)
    loads[0].wait()
    by_row = jnp.transpose(jnp.broadcast_to(gain[...], (128, rows)))[:, :1]
    up[own_rows, :] = (by_row * stage[0]).astype(jnp.bfloat16)
    pl.semaphore_wait(barrier, len(greet))

    start_own(0)
    loads[1].wait()

    def columns(owner):
        return pl.ds(pl.multiple_of(owner * width, 128), width)

    def token_copy(owner, to, slot):
        return pltpu.make_async_remote_copy(
            src_ref=tok.at[:, columns(owner)],
            dst_ref=tok.at[:, columns(owner)],
            send_sem=tok_send.at[slot], recv_sem=tok_recv.at[owner],
            device_id={"tp": to}, device_id_type=MESH)

    across = [lax.rem(group + g, groups) * 2 + core for g in range(1, groups)]
    back = [lax.rem(group + groups - g, groups) * 2 + core for g in range(1, groups)]
    token_sends = [token_copy(me, to, i) for i, to in enumerate(across)]
    token_sends.append(token_copy(me, partner, groups - 1))
    for c in token_sends:
        c.start()
    loads[2].wait()
    down[own_rows, :] = stage[1].astype(jnp.bfloat16)

    arrived(0, z * 2 + 1 - y, extra)
    relay_own_extra(0, lambda c: c.start())
    step_sends(0, 1, lambda c: c.start(), True)

    relays = []
    for i, owner in enumerate(back):
        token_copy(owner, partner, groups + i).wait_recv()
        c = token_copy(owner, partner, groups + i)
        c.start()
        relays.append(c)
    token_copy(partner, partner, 0).wait_recv()
    for g in range(1, groups):
        token_copy(lax.rem(group + g, groups) * 2 + 1 - core, partner, 0).wait_recv()
    for c in token_sends + relays:
        c.wait_send()
    tile = 128

    @pl.loop(0, tokens // tile)
    def _(i):
        at = pl.ds(pl.multiple_of(i * tile, tile), tile)
        wide = tok[at, :].astype(jnp.float32)
        scale = lax.rsqrt(jnp.mean(wide * wide, axis=-1, keepdims=True) + epsilon)
        tok[at, :] = (wide * scale).astype(jnp.bfloat16)

    for d in range(2, chain):
        step_sends(0, d, lambda c: c.start(), True)
    start_own(1)
    for d in range(chain):
        side_arrivals(0, d)
    bm, bn = min(512, tokens), min(512, units)

    def expand(first, last):
        @pl.loop(first, last)
        def _(j):
            cols = pl.ds(pl.multiple_of(j * bn, bn), bn)

            @pl.loop(0, tokens // bm)
            def _(i):
                at = pl.ds(pl.multiple_of(i * bm, bm), bm)
                values = jnp.dot(tok[at, :], up[:, cols], preferred_element_type=jnp.float32)
                values = jnp.maximum(values, 0.0)
                hidden[at, cols] = (values * values).astype(jnp.bfloat16)

    expand(0, units // bn // 2)
    arrived(1, z * 2 + 1 - y, extra)
    relay_own_extra(1, lambda c: c.start())
    step_sends(1, 1, lambda c: c.start(), True)
    expand(units // bn // 2, units // bn)

    def pair_copy(r, h):
        return pltpu.make_async_remote_copy(
            src_ref=part.at[r, h], dst_ref=pair.at[r, h], send_sem=pair_send.at[r, h], recv_sem=pair_recv.at[r, h],
            device_id={"tp": partner}, device_id_type=MESH)

    def cross_copy(r, h, to_group, from_group):
        slot = r % per_owner
        return pltpu.make_async_remote_copy(
            src_ref=part.at[r, h], dst_ref=cross.at[from_group, slot, h],
            send_sem=cross_send.at[r, h], recv_sem=cross_recv.at[from_group, slot, h],
            device_id={"tp": to_group * 2 + core}, device_id_type=MESH)

    def multiply(r, hs):
        where = pl.ds(pl.multiple_of(r * rows + hs[0] * half_rows, 16), len(hs) * half_rows)

        @pl.loop(0, tokens // bm)
        def _(i):
            at = pl.ds(pl.multiple_of(i * bm, bm), bm)
            values = lax.dot_general(
                hidden[at, :], down[where, :], (((1,), (1,)), ((), ())),
                preferred_element_type=jnp.float32).astype(jnp.bfloat16)
            for i_h, h in enumerate(hs):
                part[r, h, at, :] = values[:, i_h * half_rows:(i_h + 1) * half_rows]

        @pl.when(r // per_owner % 2 != core)
        def _():
            for h in hs:
                pair_copy(r, h).start()

    def pair_sum(r, hs):
        owner = r // per_owner

        @pl.when(owner % 2 == core)
        def _():
            for h in hs:
                pair_copy(r, h).wait_recv()

                @pl.loop(0, tokens // tile)
                def _(i):
                    at = pl.ds(pl.multiple_of(i * tile, tile), tile)
                    both = part[r, h, at, :].astype(jnp.float32) + pair[r, h, at, :].astype(jnp.float32)
                    part[r, h, at, :] = both.astype(jnp.bfloat16)

                @pl.when(owner // 2 != group)
                def _():
                    cross_copy(r, h, owner // 2, group).start()

    def at_distance(d, flip, fn):
        for sign in (-1, 1):
            at = z + sign * d

            @pl.when((at >= 0) & (at < chain))
            def _():
                fn(at * 2 + (y + flip) % 2)

    every = list(range(halves))

    def side_block(r):
        for h in every:
            arrived(1, r, h)
            multiply(r, [h])
            pair_sum(r, [h])

    multiply(fs, every)
    side_block(z * 2 + 1 - y)
    pair_sum(fs, every)
    at_distance(1, 0, lambda r: multiply(r, every))

    @pl.loop(2, chain)
    def _(d):
        step_sends(1, d, lambda c: c.start(), True)
        at_distance(d - 1, 0, lambda r: pair_sum(r, every))
        at_distance(d - 1, 1, side_block)
        at_distance(d, 0, lambda r: multiply(r, every))

    at_distance(chain - 1, 0, lambda r: pair_sum(r, every))
    at_distance(chain - 1, 1, side_block)

    for s in range(per_owner):
        r = me * per_owner + s
        for h in every:
            for g in range(1, groups):
                other = lax.rem(group + g, groups)
                cross_copy(r, h, other, other).wait_recv()

            @pl.loop(0, tokens // tile)
            def _(i):
                at = pl.ds(pl.multiple_of(i * tile, tile), tile)
                value = part[r, h, at, :].astype(jnp.float32)
                for g in range(1, groups):
                    value = value + cross[lax.rem(group + g, groups), s, h, at, :].astype(jnp.float32)
                first = s * rows + h * half_rows
                total[at, first:first + half_rows] = value.astype(jnp.bfloat16)

    for m in (0, 1):
        for way, k in own_sends(m):
            when_way(way, lambda way=way, k=k: copy(m, fs, k, way).wait_send())
        relay_own_extra(m, lambda c: c.wait_send())

        @pl.loop(1, chain)
        def _(d):
            step_sends(m, d, lambda c: c.wait_send(), False)

    @pl.loop(0, n)
    def _(r):
        owner = r // per_owner

        @pl.when(owner % 2 != core)
        def _():
            for h in every:
                pair_copy(r, h).wait_send()

        @pl.when((owner % 2 == core) & (owner // 2 != group))
        def _():
            for h in every:
                cross_copy(r, h, owner // 2, group).wait_send()


def on_device(n, tp, tokens, norm_gain, up_weight, down_weight):
    rows, units = up_weight.shape
    count, width = tokens.shape
    bf16 = jnp.bfloat16
    groups, per_owner = tp // 2, n // tp
    chunks = len(chunks_of(rows, 0))
    halves = chunks - 1
    half_rows = rows // halves
    features = width * tp
    dma = pltpu.SemaphoreType.DMA
    flops = 2 * 2 * count * features * units
    return tuple(pl.pallas_call(
        functools.partial(kernel, n, tp),
        out_shape=(pltpu.VMEM((features, units), bf16), pltpu.VMEM((features, units), bf16),
                   pltpu.VMEM((count, width), bf16)),
        in_specs=[pl.BlockSpec(memory_space=pl.ANY if i != 1 else pltpu.VMEM) for i in range(4)],
        out_specs=[pl.BlockSpec(memory_space=pltpu.VMEM)] * 3,
        scratch_shapes=[
            pltpu.VMEM((2, rows, units), jnp.float32),
            pltpu.VMEM((count, features), bf16),
            pltpu.VMEM((count, units), bf16),
            pltpu.VMEM((n, halves, count, half_rows), bf16),
            pltpu.VMEM((n, halves, count, half_rows), bf16),
            pltpu.VMEM((groups, per_owner, halves, count, half_rows), bf16),
            dma((2, 3, n, chunks)), dma((2, n, chunks)),
            dma((2 * groups,)), dma((tp,)),
            dma((n, halves)), dma((n, halves)), dma((n, halves)), dma((groups, per_owner, halves)),
            dma((3,)),
        ],
        cost_estimate=pl.CostEstimate(flops=flops, bytes_accessed=4 * features * units * 2, transcendentals=0),
        compiler_params=pltpu.CompilerParams(
            collective_id=0, has_side_effects=True, vmem_limit_bytes=44 << 20),
    )(tokens, norm_gain[None, :], up_weight, down_weight))


def solution(mesh):
    return jax.shard_map(
        functools.partial(on_device, mesh.shape["fs"], mesh.shape["tp"]),
        mesh=mesh,
        in_specs=(P("fs", "tp"), P("fs"), P("fs", "tp"), P("fs", "tp")),
        out_specs=(P(None, "tp"), P(None, "tp"), P("fs", "tp")),
        check_vma=False,
    )
```

profile of v0, /device:TPU:7, one launch (start us, length us, event | category | flops | bytes accessed | tf_op | source)
XLA Modules:
  0.0 208.5 jit_solution(3740334233674571696)
XLA Ops:
  0.6 199.9 %shard_map.67 = (bf16[2048,2048]{1,0:T(8,128)(2,1)S(1)}, bf16[2048,2048]{1,0:T(8,128)(2,1)S(1)}, bf16[1536,512]{1,0:T(8,128)(2,1)S(1)}) custom-call(bf16[1536,512]{1,0:T(8,128)(2,1)} %tok_in.1, f32[1,256]{1,0:T(1,128)} %bitcast.1, f32[256,2048]{1,0:T(8,128)} %up_weight.1, f32[256,2048]{1,0:T(8,128)} %down_weight.1), custom_call_target="tpu_custom_call" | custom-call | flops 25769803776 | bytes 33554432 | tf_op jit(solution)/shard_map/pallas_call | solution.py:334
  200.6 3.4 %copy.10 = bf16[2048,2048]{1,0:T(8,128)(2,1)} copy(bf16[2048,2048]{1,0:T(8,128)(2,1)S(1)} %get-tuple-element.3) | data formatting | bytes 16777216
  204.0 1.1 copy.12
  205.1 3.4 %copy.11 = bf16[2048,2048]{1,0:T(8,128)(2,1)} copy(bf16[2048,2048]{1,0:T(8,128)(2,1)S(1)} %get-tuple-element.4) | data formatting | bytes 16777216
where the time goes:
time: 209 us
  Pallas kernels  200 us (96%)
  local copies, waits for them, and re-layouts  7.94 us (4%)
    pallas_call x1, Pallas kernels, on_device(): pl.pallas_call(functools.partial(kernel, n, tp), out_shape=(pltpu.VMEM((f...  200 us
    unnamed x3, local copies, waits for them, and re-layouts  7.94 us

commit v1 on v0

--- a/solution.py
+++ b/solution.py
@@ -54,7 +54,7 @@
         return pltpu.make_async_remote_copy(
             src_ref=bufs[m].at[where],
             dst_ref=bufs[m].at[where],
-            send_sem=send_sem.at[m, way, src, k],
+            send_sem=send_sem.at[m, way],
             recv_sem=recv_sem.at[m, src, k],
             device_id=target(way),
             device_id_type=MESH,
@@ -64,13 +64,12 @@
         where = spot(m, src, k)
         pltpu.make_async_remote_copy(
             src_ref=bufs[m].at[where], dst_ref=bufs[m].at[where],
-            send_sem=send_sem.at[m, SIDE, src, k], recv_sem=recv_sem.at[m, src, k],
+            send_sem=send_sem.at[m, SIDE], recv_sem=recv_sem.at[m, src, k],
             device_id=target(SIDE), device_id_type=MESH,
         ).wait_recv()
 
-    def own_sends(m):
-        order = [(SIDE, extra)] + [(way, k) for k in mains for way in (UP, DOWN, SIDE)] + [(UP, extra), (DOWN, extra)]
-        return [(way, k) for way, k in order]
+    along = [(way, k) for k in mains for way in (UP, DOWN)]
+    beside = [(SIDE, extra)] + [(SIDE, k) for k in mains]
 
     def when_way(way, fn):
         if way == UP:
@@ -80,17 +79,25 @@
         else:
             fn()
 
-    def start_own(m):
-        for way, k in own_sends(m):
+    def start_own(m, order):
+        for way, k in order:
             when_way(way, lambda way=way, k=k: copy(m, fs, k, way).start())
 
-    def relay_own_extra(m, act):
-        other = z * 2 + 1 - y
+    middle = (z > 0) & (z < chain - 1)
+    opposite = z * 2 + 1 - y
+
+    def own_extras(m, late):
         for way in (UP, DOWN):
-            when_way(way, lambda way=way: act(copy(m, other, extra, way)))
-
-    def step_sends(m, d, act, wait):
-        plan = [(k, 0) for k in mains] + [(extra, 0), (extra, 1)]
+            edge = middle & (z == (chain - 2 if way == UP else 1))
+            now = edge if late else jnp.logical_not(edge)
+
+            def send(way=way):
+                copy(m, fs, extra, way).start()
+                copy(m, opposite, extra, way).start()
+
+            when_way(way, lambda now=now, send=send: pl.when(now)(send))
+
+    def step_sends(m, d, act, wait, plan):
         for k, flip in plan:
             for sign, way in ((-1, UP), (1, DOWN)):
                 at = z + sign * d
@@ -113,6 +120,12 @@
                 for k in mains:
                     arrived(m, at * 2 + 1 - y, k)
 
+    main_plan = [(k, 0) for k in mains]
+    extra_plan = [(extra, 0), (extra, 1)]
+
+    def forward(m, d, plan):
+        step_sends(m, d, lambda c: c.start(), True, plan)
+
     own_rows = pl.ds(pl.multiple_of(fs * rows, 16), rows)
     loads = [pltpu.make_async_copy(up_weight, stage.at[0], local_sem.at[1]),
              pltpu.make_async_copy(tok_in, tok.at[:, pl.ds(pl.multiple_of(me * width, 128), width)], local_sem.at[0]),
@@ -121,17 +134,23 @@
         load.start()
 
     barrier = pltpu.get_barrier_semaphore()
-    greet = [{"fs": lax.rem(z + 1, chain) * 2 + y}, {"fs": lax.rem(z + chain - 1, chain) * 2 + y},
-             {"fs": z * 2 + 1 - y}, {"tp": partner}]
+    greet = [target(SIDE), {"tp": partner}]
     greet += [{"tp": lax.rem(group + g, groups) * 2 + core} for g in range(1, groups)]
+
+    def hello(who):
+        pl.semaphore_signal(barrier, inc=1, device_id=who, device_id_type=MESH)
+
+    for way in (UP, DOWN):
+        when_way(way, lambda way=way: hello(target(way)))
     for who in greet:
-        pl.semaphore_signal(barrier, inc=1, device_id=who, device_id_type=MESH)
+        hello(who)
+    callers = len(greet) + (z > 0).astype(jnp.int32) + (z < chain - 1).astype(jnp.int32)
     loads[0].wait()
     by_row = jnp.transpose(jnp.broadcast_to(gain[...], (128, rows)))[:, :1]
     up[own_rows, :] = (by_row * stage[0]).astype(jnp.bfloat16)
-    pl.semaphore_wait(barrier, len(greet))
-
-    start_own(0)
+    pl.semaphore_wait(barrier, callers)
+
+    start_own(0, [(way, k) for k in mains for way in (UP, DOWN, SIDE)] + [(SIDE, extra)])
     loads[1].wait()
 
     def columns(owner):
@@ -153,9 +172,11 @@
     loads[2].wait()
     down[own_rows, :] = stage[1].astype(jnp.bfloat16)
 
-    arrived(0, z * 2 + 1 - y, extra)
-    relay_own_extra(0, lambda c: c.start())
-    step_sends(0, 1, lambda c: c.start(), True)
+    forward(0, 1, main_plan)
+    arrived(0, opposite, extra)
+    own_extras(0, False)
+    own_extras(0, True)
+    pl.when(jnp.logical_not(middle))(lambda: start_own(1, along))
 
     relays = []
     for i, owner in enumerate(back):
@@ -163,6 +184,7 @@
         c = token_copy(owner, partner, groups + i)
         c.start()
         relays.append(c)
+    forward(0, 2, main_plan)
     token_copy(partner, partner, 0).wait_recv()
     for g in range(1, groups):
         token_copy(lax.rem(group + g, groups) * 2 + 1 - core, partner, 0).wait_recv()
@@ -177,9 +199,12 @@
         scale = lax.rsqrt(jnp.mean(wide * wide, axis=-1, keepdims=True) + epsilon)
         tok[at, :] = (wide * scale).astype(jnp.bfloat16)
 
-    for d in range(2, chain):
-        step_sends(0, d, lambda c: c.start(), True)
-    start_own(1)
+    for d in range(3, chain):
+        forward(0, d, main_plan)
+    start_own(1, beside)
+    for d in range(1, chain):
+        forward(0, d, extra_plan)
+    pl.when(middle)(lambda: start_own(1, along))
     for d in range(chain):
         side_arrivals(0, d)
     bm, bn = min(512, tokens), min(512, units)
@@ -196,22 +221,25 @@
                 values = jnp.maximum(values, 0.0)
                 hidden[at, cols] = (values * values).astype(jnp.bfloat16)
 
-    expand(0, units // bn // 2)
-    arrived(1, z * 2 + 1 - y, extra)
-    relay_own_extra(1, lambda c: c.start())
-    step_sends(1, 1, lambda c: c.start(), True)
-    expand(units // bn // 2, units // bn)
+    parts = units // bn
+    expand(0, parts // 2)
+    arrived(1, opposite, extra)
+    own_extras(1, False)
+    forward(1, 1, main_plan[:1])
+    expand(parts // 2, parts * 3 // 4)
+    forward(1, 1, main_plan[1:])
+    expand(parts * 3 // 4, parts)
 
     def pair_copy(r, h):
         return pltpu.make_async_remote_copy(
-            src_ref=part.at[r, h], dst_ref=pair.at[r, h], send_sem=pair_send.at[r, h], recv_sem=pair_recv.at[r, h],
+            src_ref=part.at[r, h], dst_ref=pair.at[r, h], send_sem=pair_send.at[0], recv_sem=pair_recv.at[r, h],
             device_id={"tp": partner}, device_id_type=MESH)
 
     def cross_copy(r, h, to_group, from_group):
         slot = r % per_owner
         return pltpu.make_async_remote_copy(
             src_ref=part.at[r, h], dst_ref=cross.at[from_group, slot, h],
-            send_sem=cross_send.at[r, h], recv_sem=cross_recv.at[from_group, slot, h],
+            send_sem=cross_send.at[0], recv_sem=cross_recv.at[from_group, slot, h],
             device_id={"tp": to_group * 2 + core}, device_id_type=MESH)
 
     def multiply(r, hs):
@@ -259,26 +287,135 @@
 
     every = list(range(halves))
 
-    def side_block(r):
-        for h in every:
-            arrived(1, r, h)
-            multiply(r, [h])
-            pair_sum(r, [h])
+    first, rest = every[:1], every[1:]
+    last = chain - 1
+    head, tail = (first, rest) if rest else ([], every)
+
+    def opposite_block(h):
+        arrived(1, opposite, h)
+        multiply(opposite, [h])
+
+    def near_flow():
+        def side(d, hs):
+            def run(r):
+                for h in hs:
+                    arrived(1, r, h)
+                    multiply(r, [h])
+
+            at_distance(d, 1, run)
+
+        def sums(d, flip, hs):
+            at_distance(d, flip, lambda r: pair_sum(r, hs))
+
+        if head:
+            at_distance(1, 0, lambda r: multiply(r, head))
+
+        @pl.loop(2, last)
+        def _(d):
+            forward(1, d, main_plan)
+
+        @pl.loop(1, last)
+        def _(d):
+            forward(1, d, extra_plan)
+
+        own_extras(1, True)
+        pair_sum(opposite, first)
+        sums(1, 0, head)
+        for h in rest:
+            opposite_block(h)
+        at_distance(1, 0, lambda r: multiply(r, tail))
+        pair_sum(opposite, rest)
+
+        @pl.loop(2, last)
+        def _(d):
+            at_distance(d, 0, lambda r: multiply(r, every))
+
+        sums(1, 0, tail)
+        side(1, first)
+
+        @pl.loop(2, last)
+        def _(d):
+            sums(d, 0, every)
+
+        sums(1, 1, first)
+        side(1, rest)
+        sums(1, 1, rest)
+
+        @pl.loop(2, last)
+        def _(d):
+            side(d, first)
+            sums(d, 1, first)
+            side(d, rest)
+            sums(d, 1, rest)
+
+    def end_flow():
+        def far(d, flip):
+            return jnp.where(z == 0, d, last - d) * 2 + (y + flip) % 2
+
+        def take(d, k, flip=0):
+            r = far(d, flip)
+            arrived(1, r, k)
+            if k != extra:
+                copy(1, r, k, SIDE).start()
+
+        def main(d, hs):
+            if hs:
+                multiply(far(d, 0), hs)
+
+        def side(d, hs):
+            for h in hs:
+                arrived(1, far(d, 1), h)
+                multiply(far(d, 1), [h])
+
+        def sums(d, flip, hs):
+            pair_sum(far(d, flip), hs)
+
+        main(1, head)
+        pair_sum(opposite, first)
+        for h in rest:
+            opposite_block(h)
+        sums(1, 0, head)
+        pair_sum(opposite, rest)
+
+        @pl.loop(2, chain)
+        def _(d):
+            take(d, 0)
+            main(d, head)
+            side(d - 1, head)
+            sums(d, 0, head)
+            for k in mains[1:]:
+                take(d, k)
+            sums(d - 1, 1, head)
+
+        @pl.loop(2, last)
+        def _(d):
+            take(d, extra)
+            main(d, tail)
+            take(d, extra, 1)
+            sums(d, 0, tail)
+            side(d, tail)
+            sums(d, 1, tail)
+
+        take(last, extra)
+        main(last, tail)
+        take(last, extra, 1)
+        sums(last, 0, tail)
+        side(last, head)
+        take(1, extra)
+        main(1, tail)
+        sums(last, 1, head)
+        take(1, extra, 1)
+        sums(1, 0, tail)
+        side(1, tail)
+        side(last, tail)
+        sums(1, 1, tail)
+        sums(last, 1, tail)
 
     multiply(fs, every)
-    side_block(z * 2 + 1 - y)
+    opposite_block(0)
     pair_sum(fs, every)
-    at_distance(1, 0, lambda r: multiply(r, every))
-
-    @pl.loop(2, chain)
-    def _(d):
-        step_sends(1, d, lambda c: c.start(), True)
-        at_distance(d - 1, 0, lambda r: pair_sum(r, every))
-        at_distance(d - 1, 1, side_block)
-        at_distance(d, 0, lambda r: multiply(r, every))
-
-    at_distance(chain - 1, 0, lambda r: pair_sum(r, every))
-    at_distance(chain - 1, 1, side_block)
+    pl.when(middle)(near_flow)
+    pl.when(jnp.logical_not(middle))(end_flow)
 
     for s in range(per_owner):
         r = me * per_owner + s
@@ -297,27 +434,45 @@
                 total[at, first:first + half_rows] = value.astype(jnp.bfloat16)
 
     for m in (0, 1):
-        for way, k in own_sends(m):
-            when_way(way, lambda way=way, k=k: copy(m, fs, k, way).wait_send())
-        relay_own_extra(m, lambda c: c.wait_send())
-
-        @pl.loop(1, chain)
-        def _(d):
-            step_sends(m, d, lambda c: c.wait_send(), False)
-
-    @pl.loop(0, n)
-    def _(r):
-        owner = r // per_owner
-
-        @pl.when(owner % 2 != core)
-        def _():
-            for h in every:
-                pair_copy(r, h).wait_send()
-
-        @pl.when((owner % 2 == core) & (owner // 2 != group))
-        def _():
-            for h in every:
-                cross_copy(r, h, owner // 2, group).wait_send()
+        spread = rows + chunks[m][extra][1]
+
+        def sent(way, count):
+            where = pl.ds(0, count)
+            pltpu.make_async_remote_copy(
+                src_ref=bufs[m].at[where], dst_ref=bufs[m].at[where],
+                send_sem=send_sem.at[m, way], recv_sem=recv_sem.at[m, fs, 0],
+                device_id=target(way), device_id_type=MESH).wait_send()
+
+        sent(SIDE, rows + (chain - 1) * (rows - chunks[m][extra][1]))
+        for i in range(last):
+            pl.when(z == i)(lambda i=i: sent(UP, (i + 1) * spread))
+            pl.when(z == last - i)(lambda i=i: sent(DOWN, (i + 1) * spread))
+
+    def all_sent(sem, recv, count, who):
+        where = pl.ds(0, count)
+        pltpu.make_async_remote_copy(
+            src_ref=part.at[where], dst_ref=part.at[where], send_sem=sem, recv_sem=recv,
+            device_id={"tp": who}, device_id_type=MESH).wait_send()
+
+    all_sent(pair_send.at[0], pair_recv.at[0, 0], n // 2, partner)
+    if groups > 1:
+        all_sent(cross_send.at[0], cross_recv.at[0, 0, 0], per_owner * (groups - 1), partner)
+
+
+pieces = 4
+
+
+def store(up, down, total, up_out, down_out, total_out, sem):
+    copies = []
+    for i, (src, dst) in enumerate(((up, up_out), (down, down_out), (total, total_out))):
+        step = src.shape[0] // pieces
+        for j in range(pieces):
+            at = pl.ds(j * step, step)
+            copies.append(pltpu.make_async_copy(src.at[at], dst.at[at], sem.at[i, j]))
+    for c in copies:
+        c.start()
+    for c in copies:
+        c.wait()
 
 
 def on_device(n, tp, tokens, norm_gain, up_weight, down_weight):
@@ -331,7 +486,7 @@
     features = width * tp
     dma = pltpu.SemaphoreType.DMA
     flops = 2 * 2 * count * features * units
-    return tuple(pl.pallas_call(
+    results = pl.pallas_call(
         functools.partial(kernel, n, tp),
         out_shape=(pltpu.VMEM((features, units), bf16), pltpu.VMEM((features, units), bf16),
                    pltpu.VMEM((count, width), bf16)),
@@ -344,15 +499,23 @@
             pltpu.VMEM((n, halves, count, half_rows), bf16),
             pltpu.VMEM((n, halves, count, half_rows), bf16),
             pltpu.VMEM((groups, per_owner, halves, count, half_rows), bf16),
-            dma((2, 3, n, chunks)), dma((2, n, chunks)),
+            dma((2, 3)), dma((2, n, chunks)),
             dma((2 * groups,)), dma((tp,)),
-            dma((n, halves)), dma((n, halves)), dma((n, halves)), dma((groups, per_owner, halves)),
+            dma((1,)), dma((n, halves)), dma((1,)), dma((groups, per_owner, halves)),
             dma((3,)),
         ],
         cost_estimate=pl.CostEstimate(flops=flops, bytes_accessed=4 * features * units * 2, transcendentals=0),
         compiler_params=pltpu.CompilerParams(
             collective_id=0, has_side_effects=True, vmem_limit_bytes=44 << 20),
-    )(tokens, norm_gain[None, :], up_weight, down_weight))
+    )(tokens, norm_gain[None, :], up_weight, down_weight)
+    return tuple(pl.pallas_call(
+        store,
+        out_shape=[jax.ShapeDtypeStruct(r.shape, r.dtype) for r in results],
+        in_specs=[pl.BlockSpec(memory_space=pl.ANY)] * 3,
+        out_specs=[pl.BlockSpec(memory_space=pltpu.HBM)] * 3,
+        scratch_shapes=[dma((3, pieces))],
+        compiler_params=pltpu.CompilerParams(vmem_limit_bytes=1 << 20),
+    )(*results))
 
 
 def solution(mesh):

time: 209 us -> 184 us (0.88); the launches traced: 209 us -> 181 us
  Pallas kernels: 200 us -> 181 us
  local copies, waits for them, and re-layouts: 7.94 us -> 0 us
    pallas_call x1, Pallas kernels: 200 us -> 174 us  [on_device(): pl.pallas_call(functools.partial(kernel, n, tp), out_shape=(pltpu.VMEM((f...]
    unnamed x3 -> x0, local copies, waits for them, and re-layouts: 7.94 us -> none
    pallas_call x0 -> x1, Pallas kernels: none -> 6.37 us  [on_device(): pl.pallas_call(store, out_shape=[jax.ShapeDtypeStruct(r.shape, r.dtype) f...]
where the time goes in v1:
time: 184 us; the launch traced here: 181 us
  Pallas kernels  181 us (98%)
    pallas_call x1, Pallas kernels, on_device(): pl.pallas_call(functools.partial(kernel, n, tp), out_shape=(pltpu.VMEM((f...  174 us
    pallas_call x1, Pallas kernels, on_device(): pl.pallas_call(store, out_shape=[jax.ShapeDtypeStruct(r.shape, r.dtype) f...  6.37 us

profile of v1, /device:TPU:7, one launch (start us, length us, event | category | flops | bytes accessed | tf_op | source)
XLA Modules:
  0.0 181.4 jit_solution(10238813373288457993)
XLA Ops:
  0.6 174.2 %shard_map.67 = (bf16[2048,2048]{1,0:T(8,128)(2,1)S(1)}, bf16[2048,2048]{1,0:T(8,128)(2,1)S(1)}, bf16[1536,512]{1,0:T(8,128)(2,1)S(1)}) custom-call(bf16[1536,512]{1,0:T(8,128)(2,1)} %tok_in.1, f32[1,256]{1,0:T(1,128)} %bitcast.1, f32[256,2048]{1,0:T(8,128)} %up_weight.1, f32[256,2048]{1,0:T(8,128)} %down_weight.1), custom_call_target="tpu_custom_call" | custom-call | flops 25769803776 | bytes 33554432 | tf_op jit(solution)/shard_map/pallas_call | solution.py:489
  174.8 6.4 %shard_map.68 = (bf16[2048,2048]{1,0:T(8,128)(2,1)}, bf16[2048,2048]{1,0:T(8,128)(2,1)}, bf16[1536,512]{1,0:T(8,128)(2,1)}) custom-call(bf16[2048,2048]{1,0:T(8,128)(2,1)S(1)} %get-tuple-element.6.up, bf16[2048,2048]{1,0:T(8,128)(2,1)S(1)} %get-tuple-element.7.down, bf16[1536,512]{1,0:T(8,128)(2,1)S(1)} %get-tuple-element.8.total), custom_call_target="tpu_custom_call" | custom-call | tf_op jit(solution)/shard_map/pallas_call | solution.py:511

commit v2 on v1

--- a/solution.py
+++ b/solution.py
@@ -127,10 +127,13 @@
         step_sends(m, d, lambda c: c.start(), True, plan)
 
     own_rows = pl.ds(pl.multiple_of(fs * rows, 16), rows)
-    loads = [pltpu.make_async_copy(up_weight, stage.at[0], local_sem.at[1]),
-             pltpu.make_async_copy(tok_in, tok.at[:, pl.ds(pl.multiple_of(me * width, 128), width)], local_sem.at[0]),
-             pltpu.make_async_copy(down_weight, stage.at[1], local_sem.at[2])]
-    for load in loads:
+    lead = chunks[0][0][1]
+    lead_rows, other_rows = pl.ds(0, lead), pl.ds(lead, rows - lead)
+    loads = [pltpu.make_async_copy(up_weight.at[lead_rows], stage.at[0, lead_rows], local_sem.at[0]),
+             pltpu.make_async_copy(up_weight.at[other_rows], stage.at[0, other_rows], local_sem.at[1]),
+             pltpu.make_async_copy(tok_in, tok.at[:, pl.ds(pl.multiple_of(me * width, 128), width)], local_sem.at[2]),
+             pltpu.make_async_copy(down_weight, stage.at[1], local_sem.at[3])]
+    for load in loads[:2]:
         load.start()
 
     barrier = pltpu.get_barrier_semaphore()
@@ -145,13 +148,22 @@
     for who in greet:
         hello(who)
     callers = len(greet) + (z > 0).astype(jnp.int32) + (z < chain - 1).astype(jnp.int32)
+    by_row = jnp.transpose(jnp.broadcast_to(gain[...], (128, rows)))[:, :1]
+
+    def scaled(first, count):
+        at = pl.ds(pl.multiple_of(fs * rows + first, 16), count)
+        up[at, :] = (by_row[first:first + count] * stage[0, first:first + count]).astype(jnp.bfloat16)
+
     loads[0].wait()
-    by_row = jnp.transpose(jnp.broadcast_to(gain[...], (128, rows)))[:, :1]
-    up[own_rows, :] = (by_row * stage[0]).astype(jnp.bfloat16)
+    for load in loads[2:]:
+        load.start()
+    scaled(0, lead)
     pl.semaphore_wait(barrier, callers)
-
-    start_own(0, [(way, k) for k in mains for way in (UP, DOWN, SIDE)] + [(SIDE, extra)])
+    start_own(0, [(way, 0) for way in (UP, DOWN, SIDE)])
     loads[1].wait()
+    scaled(lead, rows - lead)
+    start_own(0, [(way, k) for k in mains[1:] for way in (UP, DOWN, SIDE)] + [(SIDE, extra)])
+    loads[2].wait()
 
     def columns(owner):
         return pl.ds(pl.multiple_of(owner * width, 128), width)
@@ -169,7 +181,7 @@
     token_sends.append(token_copy(me, partner, groups - 1))
     for c in token_sends:
         c.start()
-    loads[2].wait()
+    loads[3].wait()
     down[own_rows, :] = stage[1].astype(jnp.bfloat16)
 
     forward(0, 1, main_plan)
@@ -230,52 +242,64 @@
     forward(1, 1, main_plan[1:])
     expand(parts * 3 // 4, parts)
 
-    def pair_copy(r, h):
+    tiles = tokens // bm
+
+    def tile_rows(i):
+        return pl.ds(pl.multiple_of(i * bm, bm), bm)
+
+    def pair_copy(r, h, i):
         return pltpu.make_async_remote_copy(
-            src_ref=part.at[r, h], dst_ref=pair.at[r, h], send_sem=pair_send.at[0], recv_sem=pair_recv.at[r, h],
+            src_ref=part.at[r, h, tile_rows(i)], dst_ref=pair.at[r, h, tile_rows(i)],
+            send_sem=pair_send.at[0], recv_sem=pair_recv.at[r, h, i],
             device_id={"tp": partner}, device_id_type=MESH)
 
-    def cross_copy(r, h, to_group, from_group):
+    def cross_copy(r, h, i, to_group, from_group):
         slot = r % per_owner
         return pltpu.make_async_remote_copy(
-            src_ref=part.at[r, h], dst_ref=cross.at[from_group, slot, h],
-            send_sem=cross_send.at[0], recv_sem=cross_recv.at[from_group, slot, h],
+            src_ref=part.at[r, h, tile_rows(i)], dst_ref=cross.at[from_group, slot, h, tile_rows(i)],
+            send_sem=cross_send.at[0], recv_sem=cross_recv.at[from_group, slot, h, i],
             device_id={"tp": to_group * 2 + core}, device_id_type=MESH)
 
-    def multiply(r, hs):
+    def multiply(r, hs, after=lambda i: None):
         where = pl.ds(pl.multiple_of(r * rows + hs[0] * half_rows, 16), len(hs) * half_rows)
 
-        @pl.loop(0, tokens // bm)
+        @pl.loop(0, tiles)
         def _(i):
-            at = pl.ds(pl.multiple_of(i * bm, bm), bm)
+            at = tile_rows(i)
             values = lax.dot_general(
                 hidden[at, :], down[where, :], (((1,), (1,)), ((), ())),
                 preferred_element_type=jnp.float32).astype(jnp.bfloat16)
             for i_h, h in enumerate(hs):
                 part[r, h, at, :] = values[:, i_h * half_rows:(i_h + 1) * half_rows]
 
-        @pl.when(r // per_owner % 2 != core)
-        def _():
-            for h in hs:
-                pair_copy(r, h).start()
-
-    def pair_sum(r, hs):
+            @pl.when(r // per_owner % 2 != core)
+            def _():
+                for h in hs:
+                    pair_copy(r, h, i).start()
+
+            after(i)
+
+    def pair_tile(r, hs, i):
         owner = r // per_owner
 
         @pl.when(owner % 2 == core)
         def _():
+            at = tile_rows(i)
             for h in hs:
-                pair_copy(r, h).wait_recv()
-
-                @pl.loop(0, tokens // tile)
-                def _(i):
-                    at = pl.ds(pl.multiple_of(i * tile, tile), tile)
-                    both = part[r, h, at, :].astype(jnp.float32) + pair[r, h, at, :].astype(jnp.float32)
-                    part[r, h, at, :] = both.astype(jnp.bfloat16)
-
-                @pl.when(owner // 2 != group)
-                def _():
-                    cross_copy(r, h, owner // 2, group).start()
+                pair_copy(r, h, i).wait_recv()
+                both = part[r, h, at, :].astype(jnp.float32) + pair[r, h, at, :].astype(jnp.float32)
+                part[r, h, at, :] = both.astype(jnp.bfloat16)
+                pl.when(owner // 2 != group)(lambda h=h: cross_copy(r, h, i, owner // 2, group).start())
+
+    def pair_sum(r, hs):
+        if hs:
+            pl.loop(0, tiles)(lambda i: pair_tile(r, hs, i))
+
+    def eager(r, hs):
+        return lambda i: pl.when(core == 0)(lambda: pair_tile(r, hs, i))
+
+    def later(r, hs):
+        pl.when(core == 1)(lambda: pair_sum(r, hs))
 
     def at_distance(d, flip, fn):
         for sign in (-1, 1):
@@ -289,11 +313,23 @@
 
     first, rest = every[:1], every[1:]
     last = chain - 1
+    outer = (z <= 1) | (z >= last - 1)
+    final = jnp.where(z <= 1, last, 0) * 2 + 1 - y
     head, tail = (first, rest) if rest else ([], every)
 
     def opposite_block(h):
         arrived(1, opposite, h)
         multiply(opposite, [h])
+
+    def final_block(meanwhile):
+        h = every[-1]
+
+        def after(i):
+            pl.when(core == 0)(lambda: pair_tile(final, [h], i))
+            pl.when(core == 1)(lambda: meanwhile(i))
+
+        arrived(1, final, h)
+        multiply(final, [h], after)
 
     def near_flow():
         def side(d, hs):
@@ -314,11 +350,13 @@
         def _(d):
             forward(1, d, main_plan)
 
-        @pl.loop(1, last)
+        @pl.loop(1, last - 1)
         def _(d):
             forward(1, d, extra_plan)
 
+        forward(1, last - 1, extra_plan[:1])
         own_extras(1, True)
+        forward(1, last - 1, extra_plan[1:])
         pair_sum(opposite, first)
         sums(1, 0, head)
         for h in rest:
@@ -341,12 +379,20 @@
         side(1, rest)
         sums(1, 1, rest)
 
-        @pl.loop(2, last)
-        def _(d):
-            side(d, first)
-            sums(d, 1, first)
-            side(d, rest)
-            sums(d, 1, rest)
+        @pl.loop(2, last - 1)
+        def _(d):
+            side(d, every)
+            sums(d, 1, every)
+
+        @pl.when(outer)
+        def _():
+            before = every[:-1]
+            for h in before:
+                arrived(1, final, h)
+                multiply(final, [h], eager(final, [h]))
+            later(final, before)
+            final_block(lambda i: None)
+            later(final, every[-1:])
 
     def end_flow():
         def far(d, flip):
@@ -358,14 +404,16 @@
             if k != extra:
                 copy(1, r, k, SIDE).start()
 
-        def main(d, hs):
+        def main(d, hs, soon=False):
+            r = far(d, 0)
             if hs:
-                multiply(far(d, 0), hs)
-
-        def side(d, hs):
+                multiply(r, hs, *([eager(r, hs)] if soon else []))
+
+        def side(d, hs, soon=False):
+            r = far(d, 1)
             for h in hs:
-                arrived(1, far(d, 1), h)
-                multiply(far(d, 1), [h])
+                arrived(1, r, h)
+                multiply(r, [h], *([eager(r, [h])] if soon else []))
 
         def sums(d, flip, hs):
             pair_sum(far(d, flip), hs)
@@ -381,8 +429,8 @@
         def _(d):
             take(d, 0)
             main(d, head)
+            sums(d, 0, head)
             side(d - 1, head)
-            sums(d, 0, head)
             for k in mains[1:]:
                 take(d, k)
             sums(d - 1, 1, head)
@@ -397,19 +445,18 @@
             sums(d, 1, tail)
 
         take(last, extra)
-        main(last, tail)
+        main(last, tail, True)
+        take(1, extra)
+        main(1, tail, True)
+        later(far(last, 0), tail)
+        side(last, head, True)
+        later(far(1, 0), tail)
+        take(1, extra, 1)
+        side(1, tail, True)
+        later(final, head)
         take(last, extra, 1)
-        sums(last, 0, tail)
-        side(last, head)
-        take(1, extra)
-        main(1, tail)
-        sums(last, 1, head)
-        take(1, extra, 1)
-        sums(1, 0, tail)
-        side(1, tail)
-        side(last, tail)
-        sums(1, 1, tail)
-        sums(last, 1, tail)
+        final_block(lambda i: pair_tile(far(1, 1), tail, i))
+        later(final, every[-1:])
 
     multiply(fs, every)
     opposite_block(0)
@@ -420,18 +467,17 @@
     for s in range(per_owner):
         r = me * per_owner + s
         for h in every:
-            for g in range(1, groups):
-                other = lax.rem(group + g, groups)
-                cross_copy(r, h, other, other).wait_recv()
-
-            @pl.loop(0, tokens // tile)
+            first_column = s * rows + h * half_rows
+
+            @pl.loop(0, tiles)
             def _(i):
-                at = pl.ds(pl.multiple_of(i * tile, tile), tile)
+                at = tile_rows(i)
                 value = part[r, h, at, :].astype(jnp.float32)
                 for g in range(1, groups):
-                    value = value + cross[lax.rem(group + g, groups), s, h, at, :].astype(jnp.float32)
-                first = s * rows + h * half_rows
-                total[at, first:first + half_rows] = value.astype(jnp.bfloat16)
+                    other = lax.rem(group + g, groups)
+                    cross_copy(r, h, i, other, other).wait_recv()
+                    value = value + cross[other, s, h, at, :].astype(jnp.float32)
+                total[at, first_column:first_column + half_rows] = value.astype(jnp.bfloat16)
 
     for m in (0, 1):
         spread = rows + chunks[m][extra][1]
@@ -454,9 +500,9 @@
             src_ref=part.at[where], dst_ref=part.at[where], send_sem=sem, recv_sem=recv,
             device_id={"tp": who}, device_id_type=MESH).wait_send()
 
-    all_sent(pair_send.at[0], pair_recv.at[0, 0], n // 2, partner)
+    all_sent(pair_send.at[0], pair_recv.at[0, 0, 0], n // 2, partner)
     if groups > 1:
-        all_sent(cross_send.at[0], cross_recv.at[0, 0, 0], per_owner * (groups - 1), partner)
+        all_sent(cross_send.at[0], cross_recv.at[0, 0, 0, 0], per_owner * (groups - 1), partner)
 
 
 pieces = 4
@@ -484,6 +530,7 @@
     halves = chunks - 1
     half_rows = rows // halves
     features = width * tp
+    tiles = count // min(512, count)
     dma = pltpu.SemaphoreType.DMA
     flops = 2 * 2 * count * features * units
     results = pl.pallas_call(
@@ -501,8 +548,8 @@
             pltpu.VMEM((groups, per_owner, halves, count, half_rows), bf16),
             dma((2, 3)), dma((2, n, chunks)),
             dma((2 * groups,)), dma((tp,)),
-            dma((1,)), dma((n, halves)), dma((1,)), dma((groups, per_owner, halves)),
-            dma((3,)),
+            dma((1,)), dma((n, halves, tiles)), dma((1,)), dma((groups, per_owner, halves, tiles)),
+            dma((4,)),
         ],
         cost_estimate=pl.CostEstimate(flops=flops, bytes_accessed=4 * features * units * 2, transcendentals=0),
         compiler_params=pltpu.CompilerParams(

time: 184 us -> 180 us (0.978)
  Pallas kernels: 181 us -> 178 us
    pallas_call x1, Pallas kernels: 174 us -> 171 us  [on_device(): pl.pallas_call(functools.partial(kernel, n, tp), out_shape=(pltpu.VMEM((f...]
where the time goes in v2:
time: 180 us; the launch traced here: 179 us
  Pallas kernels  178 us (99%)
    pallas_call x1, Pallas kernels, on_device(): pl.pallas_call(functools.partial(kernel, n, tp), out_shape=(pltpu.VMEM((f...  171 us
    pallas_call x1, Pallas kernels, on_device(): pl.pallas_call(store, out_shape=[jax.ShapeDtypeStruct(r.shape, r.dtype) f...  6.37 us

profile of v2, /device:TPU:7, one launch (start us, length us, event | category | flops | bytes accessed | tf_op | source)
XLA Modules:
  0.0 178.6 jit_solution(5663502552387561583)
XLA Ops:
  0.6 171.4 %shard_map.67 = (bf16[2048,2048]{1,0:T(8,128)(2,1)S(1)}, bf16[2048,2048]{1,0:T(8,128)(2,1)S(1)}, bf16[1536,512]{1,0:T(8,128)(2,1)S(1)}) custom-call(bf16[1536,512]{1,0:T(8,128)(2,1)} %tok_in.1, f32[1,256]{1,0:T(1,128)} %bitcast.1, f32[256,2048]{1,0:T(8,128)} %up_weight.1, f32[256,2048]{1,0:T(8,128)} %down_weight.1), custom_call_target="tpu_custom_call" | custom-call | flops 25769803776 | bytes 33554432 | tf_op jit(solution)/shard_map/pallas_call | solution.py:536
  172.0 6.4 %shard_map.68 = (bf16[2048,2048]{1,0:T(8,128)(2,1)}, bf16[2048,2048]{1,0:T(8,128)(2,1)}, bf16[1536,512]{1,0:T(8,128)(2,1)}) custom-call(bf16[2048,2048]{1,0:T(8,128)(2,1)S(1)} %get-tuple-element.6.up, bf16[2048,2048]{1,0:T(8,128)(2,1)S(1)} %get-tuple-element.7.down, bf16[1536,512]{1,0:T(8,128)(2,1)S(1)} %get-tuple-element.8.total), custom_call_target="tpu_custom_call" | custom-call | tf_op jit(solution)/shard_map/pallas_call | solution.py:558

commit v3 on v2

--- a/solution.py
+++ b/solution.py
@@ -13,7 +13,7 @@
 
 
 def chunks_of(rows, m):
-    extra = max(16, rows * (2 + m) // 16 // 16 * 16)
+    extra = max(16, rows * (5 + m) // 32 // 8 * 8)
     main, half = rows - extra, rows // 2
     if half % 128 == 0:
         return [(0, half), (half, main - half), (main, extra)]
@@ -22,7 +22,7 @@
 
 def kernel(n, tp, tok_in, gain, up_weight, down_weight, up, down, total,
            stage, tok, hidden, part, pair, cross,
-           send_sem, recv_sem, tok_send, tok_recv, pair_send, pair_recv, cross_send, cross_recv, local_sem):
+           send_sem, recv_sem, tok_send, tok_recv, pair_send, pair_recv, cross_send, cross_recv, local_sem, gain_row):
     rows, units = up_weight.shape
     tokens, width = tok_in.shape
     chain = n // 2
@@ -47,7 +47,7 @@
         return {"fs": z * 2 + 1 - y}
 
     def spot(m, src, k):
-        return pl.ds(pl.multiple_of(pl.multiple_of(src * rows, 16) + chunks[m][k][0], 16), chunks[m][k][1])
+        return pl.ds(pl.multiple_of(pl.multiple_of(src * rows, 16) + chunks[m][k][0], 8), chunks[m][k][1])
 
     def copy(m, src, k, way):
         where = spot(m, src, k)
@@ -133,6 +133,8 @@
              pltpu.make_async_copy(up_weight.at[other_rows], stage.at[0, other_rows], local_sem.at[1]),
              pltpu.make_async_copy(tok_in, tok.at[:, pl.ds(pl.multiple_of(me * width, 128), width)], local_sem.at[2]),
              pltpu.make_async_copy(down_weight, stage.at[1], local_sem.at[3])]
+    gain_load = pltpu.make_async_copy(gain, gain_row, local_sem.at[4])
+    gain_load.start()
     for load in loads[:2]:
         load.start()
 
@@ -148,7 +150,8 @@
     for who in greet:
         hello(who)
     callers = len(greet) + (z > 0).astype(jnp.int32) + (z < chain - 1).astype(jnp.int32)
-    by_row = jnp.transpose(jnp.broadcast_to(gain[...], (128, rows)))[:, :1]
+    gain_load.wait()
+    by_row = jnp.transpose(jnp.broadcast_to(gain_row[...], (128, rows)))[:, :1]
 
     def scaled(first, count):
         at = pl.ds(pl.multiple_of(fs * rows + first, 16), count)
@@ -159,10 +162,13 @@
         load.start()
     scaled(0, lead)
     pl.semaphore_wait(barrier, callers)
-    start_own(0, [(way, 0) for way in (UP, DOWN, SIDE)])
+    behind = (core == 1) & (z < chain // 2)
+    leading = [(way, 0) for way in (UP, DOWN, SIDE)]
+    following = [(way, k) for k in mains[1:] for way in (UP, DOWN, SIDE)] + [(SIDE, extra)]
+    pl.when(jnp.logical_not(behind))(lambda: start_own(0, leading))
     loads[1].wait()
     scaled(lead, rows - lead)
-    start_own(0, [(way, k) for k in mains[1:] for way in (UP, DOWN, SIDE)] + [(SIDE, extra)])
+    pl.when(jnp.logical_not(behind))(lambda: start_own(0, following))
     loads[2].wait()
 
     def columns(owner):
@@ -183,6 +189,7 @@
         c.start()
     loads[3].wait()
     down[own_rows, :] = stage[1].astype(jnp.bfloat16)
+    pl.when(behind)(lambda: start_own(0, leading + following))
 
     forward(0, 1, main_plan)
     arrived(0, opposite, extra)
@@ -250,7 +257,7 @@
     def pair_copy(r, h, i):
         return pltpu.make_async_remote_copy(
             src_ref=part.at[r, h, tile_rows(i)], dst_ref=pair.at[r, h, tile_rows(i)],
-            send_sem=pair_send.at[0], recv_sem=pair_recv.at[r, h, i],
+            send_sem=pair_send.at[0], recv_sem=pair_recv.at[r // (2 * per_owner) * per_owner + r % per_owner, h, i],
             device_id={"tp": partner}, device_id_type=MESH)
 
     def cross_copy(r, h, i, to_group, from_group):
@@ -296,10 +303,7 @@
             pl.loop(0, tiles)(lambda i: pair_tile(r, hs, i))
 
     def eager(r, hs):
-        return lambda i: pl.when(core == 0)(lambda: pair_tile(r, hs, i))
-
-    def later(r, hs):
-        pl.when(core == 1)(lambda: pair_sum(r, hs))
+        return lambda i: pair_tile(r, hs, i)
 
     def at_distance(d, flip, fn):
         for sign in (-1, 1):
@@ -321,15 +325,9 @@
         arrived(1, opposite, h)
         multiply(opposite, [h])
 
-    def final_block(meanwhile):
-        h = every[-1]
-
-        def after(i):
-            pl.when(core == 0)(lambda: pair_tile(final, [h], i))
-            pl.when(core == 1)(lambda: meanwhile(i))
-
-        arrived(1, final, h)
-        multiply(final, [h], after)
+    def final_block():
+        arrived(1, final, every[-1])
+        multiply(final, every[-1:], eager(final, every[-1:]))
 
     def near_flow():
         def side(d, hs):
@@ -390,9 +388,7 @@
             for h in before:
                 arrived(1, final, h)
                 multiply(final, [h], eager(final, [h]))
-            later(final, before)
-            final_block(lambda i: None)
-            later(final, every[-1:])
+            final_block()
 
     def end_flow():
         def far(d, flip):
@@ -448,15 +444,11 @@
         main(last, tail, True)
         take(1, extra)
         main(1, tail, True)
-        later(far(last, 0), tail)
         side(last, head, True)
-        later(far(1, 0), tail)
         take(1, extra, 1)
         side(1, tail, True)
-        later(final, head)
         take(last, extra, 1)
-        final_block(lambda i: pair_tile(far(1, 1), tail, i))
-        later(final, every[-1:])
+        final_block()
 
     multiply(fs, every)
     opposite_block(0)
@@ -505,7 +497,7 @@
         all_sent(cross_send.at[0], cross_recv.at[0, 0, 0, 0], per_owner * (groups - 1), partner)
 
 
-pieces = 4
+pieces = 2
 
 
 def store(up, down, total, up_out, down_out, total_out, sem):
@@ -537,7 +529,7 @@
         functools.partial(kernel, n, tp),
         out_shape=(pltpu.VMEM((features, units), bf16), pltpu.VMEM((features, units), bf16),
                    pltpu.VMEM((count, width), bf16)),
-        in_specs=[pl.BlockSpec(memory_space=pl.ANY if i != 1 else pltpu.VMEM) for i in range(4)],
+        in_specs=[pl.BlockSpec(memory_space=pl.ANY)] * 4,
         out_specs=[pl.BlockSpec(memory_space=pltpu.VMEM)] * 3,
         scratch_shapes=[
             pltpu.VMEM((2, rows, units), jnp.float32),
@@ -548,8 +540,8 @@
             pltpu.VMEM((groups, per_owner, halves, count, half_rows), bf16),
             dma((2, 3)), dma((2, n, chunks)),
             dma((2 * groups,)), dma((tp,)),
-            dma((1,)), dma((n, halves, tiles)), dma((1,)), dma((groups, per_owner, halves, tiles)),
-            dma((4,)),
+            dma((1,)), dma((n // 2, halves, tiles)), dma((1,)), dma((groups, per_owner, halves, tiles)),
+            dma((5,)), pltpu.VMEM((1, rows), jnp.float32),
         ],
         cost_estimate=pl.CostEstimate(flops=flops, bytes_accessed=4 * features * units * 2, transcendentals=0),
         compiler_params=pltpu.CompilerParams(

time: 180 us -> 178 us (0.989)
  no operation moved by 1% of the time
where the time goes in v3:
time: 178 us
  Pallas kernels  177 us (99%)
    pallas_call x1, Pallas kernels, on_device(): pl.pallas_call(functools.partial(kernel, n, tp), out_shape=(pltpu.VMEM((f...  171 us
    pallas_call x1, Pallas kernels, on_device(): pl.pallas_call(store, out_shape=[jax.ShapeDtypeStruct(r.shape, r.dtype) f...  6.34 us

profile of v3, /device:TPU:7, one launch (start us, length us, event | category | flops | bytes accessed | tf_op | source)
XLA Modules:
  0.0 177.9 jit_solution(8926382239580737600)
XLA Ops:
  0.6 170.8 %shard_map.67 = (bf16[2048,2048]{1,0:T(8,128)(2,1)S(1)}, bf16[2048,2048]{1,0:T(8,128)(2,1)S(1)}, bf16[1536,512]{1,0:T(8,128)(2,1)S(1)}) custom-call(bf16[1536,512]{1,0:T(8,128)(2,1)} %tok_in.1, f32[1,256]{1,0:T(1,128)} %bitcast.1, f32[256,2048]{1,0:T(8,128)} %up_weight.1, f32[256,2048]{1,0:T(8,128)} %down_weight.1), custom_call_target="tpu_custom_call" | custom-call | flops 25769803776 | bytes 33554432 | tf_op jit(solution)/shard_map/pallas_call | solution.py:528
  171.4 6.3 %shard_map.68 = (bf16[2048,2048]{1,0:T(8,128)(2,1)}, bf16[2048,2048]{1,0:T(8,128)(2,1)}, bf16[1536,512]{1,0:T(8,128)(2,1)}) custom-call(bf16[2048,2048]{1,0:T(8,128)(2,1)S(1)} %get-tuple-element.6.up, bf16[2048,2048]{1,0:T(8,128)(2,1)S(1)} %get-tuple-element.7.down, bf16[1536,512]{1,0:T(8,128)(2,1)S(1)} %get-tuple-element.8.total), custom_call_target="tpu_custom_call" | custom-call | tf_op jit(solution)/shard_map/pallas_call | solution.py:550

commit v4 on v3

--- a/solution.py
+++ b/solution.py
@@ -260,11 +260,12 @@
             send_sem=pair_send.at[0], recv_sem=pair_recv.at[r // (2 * per_owner) * per_owner + r % per_owner, h, i],
             device_id={"tp": partner}, device_id_type=MESH)
 
-    def cross_copy(r, h, i, to_group, from_group):
+    def cross_copy(r, h, i, to_group, from_group, into):
         slot = r % per_owner
+        lane = lax.rem(from_group + groups - into + groups - 1, groups)
         return pltpu.make_async_remote_copy(
             src_ref=part.at[r, h, tile_rows(i)], dst_ref=cross.at[from_group, slot, h, tile_rows(i)],
-            send_sem=cross_send.at[0], recv_sem=cross_recv.at[from_group, slot, h, i],
+            send_sem=cross_send.at[0], recv_sem=cross_recv.at[lane, slot, h, i],
             device_id={"tp": to_group * 2 + core}, device_id_type=MESH)
 
     def multiply(r, hs, after=lambda i: None):
@@ -296,7 +297,7 @@
                 pair_copy(r, h, i).wait_recv()
                 both = part[r, h, at, :].astype(jnp.float32) + pair[r, h, at, :].astype(jnp.float32)
                 part[r, h, at, :] = both.astype(jnp.bfloat16)
-                pl.when(owner // 2 != group)(lambda h=h: cross_copy(r, h, i, owner // 2, group).start())
+                pl.when(owner // 2 != group)(lambda h=h: cross_copy(r, h, i, owner // 2, group, owner // 2).start())
 
     def pair_sum(r, hs):
         if hs:
@@ -467,7 +468,7 @@
                 value = part[r, h, at, :].astype(jnp.float32)
                 for g in range(1, groups):
                     other = lax.rem(group + g, groups)
-                    cross_copy(r, h, i, other, other).wait_recv()
+                    cross_copy(r, h, i, other, other, group).wait_recv()
                     value = value + cross[other, s, h, at, :].astype(jnp.float32)
                 total[at, first_column:first_column + half_rows] = value.astype(jnp.bfloat16)
 
@@ -540,7 +541,7 @@
             pltpu.VMEM((groups, per_owner, halves, count, half_rows), bf16),
             dma((2, 3)), dma((2, n, chunks)),
             dma((2 * groups,)), dma((tp,)),
-            dma((1,)), dma((n // 2, halves, tiles)), dma((1,)), dma((groups, per_owner, halves, tiles)),
+            dma((1,)), dma((n // 2, halves, tiles)), dma((1,)), dma((max(groups - 1, 1), per_owner, halves, tiles)),
             dma((5,)), pltpu.VMEM((1, rows), jnp.float32),
         ],
         cost_estimate=pl.CostEstimate(flops=flops, bytes_accessed=4 * features * units * 2, transcendentals=0),

time: 178 us -> 178 us (level)
  no operation moved by 1% of the time
where the time goes in v4:
time: 178 us
  Pallas kernels  177 us (99%)
    pallas_call x1, Pallas kernels, on_device(): pl.pallas_call(functools.partial(kernel, n, tp), out_shape=(pltpu.VMEM((f...  171 us
    pallas_call x1, Pallas kernels, on_device(): pl.pallas_call(store, out_shape=[jax.ShapeDtypeStruct(r.shape, r.dtype) f...  6.34 us

profile of v4, /device:TPU:7, one launch (start us, length us, event | category | flops | bytes accessed | tf_op | source)
XLA Modules:
  0.0 177.8 jit_solution(9312689800074250207)
XLA Ops:
  0.6 170.7 %shard_map.67 = (bf16[2048,2048]{1,0:T(8,128)(2,1)S(1)}, bf16[2048,2048]{1,0:T(8,128)(2,1)S(1)}, bf16[1536,512]{1,0:T(8,128)(2,1)S(1)}) custom-call(bf16[1536,512]{1,0:T(8,128)(2,1)} %tok_in.1, f32[1,256]{1,0:T(1,128)} %bitcast.1, f32[256,2048]{1,0:T(8,128)} %up_weight.1, f32[256,2048]{1,0:T(8,128)} %down_weight.1), custom_call_target="tpu_custom_call" | custom-call | flops 25769803776 | bytes 33554432 | tf_op jit(solution)/shard_map/pallas_call | solution.py:529
  171.3 6.3 %shard_map.68 = (bf16[2048,2048]{1,0:T(8,128)(2,1)}, bf16[2048,2048]{1,0:T(8,128)(2,1)}, bf16[1536,512]{1,0:T(8,128)(2,1)}) custom-call(bf16[2048,2048]{1,0:T(8,128)(2,1)S(1)} %get-tuple-element.6.up, bf16[2048,2048]{1,0:T(8,128)(2,1)S(1)} %get-tuple-element.7.down, bf16[1536,512]{1,0:T(8,128)(2,1)S(1)} %get-tuple-element.8.total), custom_call_target="tpu_custom_call" | custom-call | tf_op jit(solution)/shard_map/pallas_call | solution.py:551
